TPU v7x, 512 devices: a whole 4x4x16 slice. The times are simulated.
512 devices in a mesh: sp: 64 (over z, y), dp: 8 (over x, core).
Axes of the slice: x: 4, y: 4, z: 16, core: 2. Of those that a mesh axis runs over, the one named last changes fastest.
Arguments:
- signal: bfloat16 [8, 8192, 1024], P('dp', 'sp'), may hold values from -6 to 6
- pace: float32 [8, 64], P('dp'), may hold values from 0.5 to 2
- log_step: float32 [64], P('sp'), may hold values from -5.52 to -4.42
- a_real: float32 [64, 64], P('sp'), may hold values from -4 to -0.002, as said below
- a_imag: float32 [64, 64], P('sp'), may hold values from 0.5 to 201.06177
- in_map: float32 [64, 2, 64, 16], P('sp'), may hold values from -3 to 3
- out_map: float32 [64, 2, 16, 64], P('sp'), may hold values from -0.5 to 0.5
- skip: float32 [1024], P('sp'), may hold values from -1 to 1
- init_state: float32 [8, 2, 64, 64], P('dp', None, 'sp'), may hold values from -5 to 5
- w_glu: bfloat16 [1024, 1024], P('sp', 'dp'), may hold values from -0.1875 to 0.1875
- b_glu: float32 [1024], replicated, may hold values from -4 to 4
- g_mix: float32 [1024], replicated, may hold values from 0.1 to 1.9
- w_out: bfloat16 [1024, 4096], P('sp', 'dp'), may hold values from -0.1875 to 0.1875
Outputs:
- result: bfloat16 [8, 8192, 4096], P('dp', 'sp')
Inputs may be any that keep to these rules, and one draw needn't show every extreme that they name: `a_real`: negative entries; within a group all entries are of one order.
All inputs are finite; a program needn't handle non-finite values.
Results may differ from a plain program's by a relative error of at most 0.0075.
Values may be sent and summed in bfloat16 or wider, within the bound.
A program may use at most 64 MiB of HBM per device.

v0:
```python
import jax
import jax.numpy as jnp
from jax import lax
from jax.sharding import Mesh
from jax.sharding import PartitionSpec as P

SP = ("sp_0", "sp_1")


def split_up(x, dim, count):
    before, after = (x.shape[:dim], x.shape[dim + 1 :])
    return jnp.moveaxis(x.reshape(*before, count, -1, *after), dim, 0)


def in_order(pieces, dim):
    pieces = jnp.moveaxis(pieces, 0, dim)
    lengths = pieces.shape
    return pieces.reshape(*lengths[:dim], lengths[dim] * lengths[dim + 1], *lengths[dim + 2 :])


def moved_by_axis(pieces, axes, order):
    lengths = [lax.axis_size(a) for a in axes]
    pieces = pieces.reshape(*lengths, *pieces.shape[1:])
    for k in order:
        pieces = lax.all_to_all(pieces, axes[k], split_axis=k, concat_axis=k, tiled=True)
    return pieces.reshape(-1, *pieces.shape[len(axes) :])


def stepwise_exchange(x, axes, order, split_dim, concat_dim):
    pieces = split_up(x, split_dim, lax.axis_size(axes))
    return in_order(moved_by_axis(pieces, axes, order), concat_dim)


def in_one_piece(arrays, axis, dim, along):
    widths = [a.shape[along] for a in arrays]
    both = jnp.concatenate(arrays, axis=along)
    whole = lax.all_gather(both, axis, axis=dim, tiled=True)
    return tuple(jnp.split(whole, [sum(widths[:k]) for k in range(1, len(widths))], axis=along))


def from_everyone(x, axis):
    copies = jnp.broadcast_to(x, (lax.axis_size(axis), *x.shape))
    return lax.all_to_all(copies, axis, split_axis=0, concat_axis=0, tiled=True)


def gathered_copies(x, axis, dim):
    return in_order(from_everyone(x, axis), dim)


def combine(first, second):
    a1r, a1i, b1r, b1i = first
    a2r, a2i, b2r, b2i = second
    return (
        a2r * a1r - a2i * a1i,
        a2r * a1i + a2i * a1r,
        a2r * b1r - a2i * b1i + b2r,
        a2r * b1i + a2i * b1r + b2i,
    )


def mix_group(series, pace_row, log_rate, a_re, a_im, in_map, out_map, skip_row, init):
    blocks_count = pace_row.shape[0]
    length = series.shape[0]
    span = length // blocks_count
    states = a_re.shape[0]
    steps = (jnp.exp(log_rate) * pace_row)[:, None]
    decay = jnp.exp(a_re * steps)
    bar_re = decay * jnp.cos(a_im * steps)
    bar_im = decay * jnp.sin(a_im * steps)
    modulus = a_re * a_re + a_im * a_im
    coef_re = ((bar_re - 1.0) * a_re + bar_im * a_im) / modulus
    coef_im = (bar_im * a_re - (bar_re - 1.0) * a_im) / modulus
    drive_re = coef_re[..., None] * in_map[0] - coef_im[..., None] * in_map[1]
    drive_im = coef_re[..., None] * in_map[1] + coef_im[..., None] * in_map[0]
    drive = jnp.concatenate([drive_re, drive_im], axis=1).astype(jnp.bfloat16)
    blocks = series.reshape(blocks_count, span, series.shape[1])
    inject = jnp.einsum("kpc,ksc->kps", drive, blocks, preferred_element_type=jnp.float32)
    inner_re = inject[:, :states]
    inner_im = inject[:, states:]
    power_re = bar_re[..., None]
    power_im = bar_im[..., None]
    offset = 1
    while offset < span:
        moved_re = jnp.pad(inner_re[..., :-offset], ((0, 0), (0, 0), (offset, 0)))
        moved_im = jnp.pad(inner_im[..., :-offset], ((0, 0), (0, 0), (offset, 0)))
        inner_re, inner_im = (
            inner_re + power_re * moved_re - power_im * moved_im,
            inner_im + power_re * moved_im + power_im * moved_re,
        )
        power_re, power_im = (power_re * power_re - power_im * power_im, 2.0 * power_re * power_im)
        offset = offset * 2
    ends_re = (
        inner_re[:, :, -1].at[0].add(power_re[0, :, 0] * init[0] - power_im[0, :, 0] * init[1])
    )
    ends_im = (
        inner_im[:, :, -1].at[0].add(power_re[0, :, 0] * init[1] + power_im[0, :, 0] * init[0])
    )
    carried = lax.associative_scan(
        combine, (power_re[..., 0], power_im[..., 0], ends_re, ends_im), axis=0
    )
    before_re = jnp.concatenate([init[0][None], carried[2][:-1]], axis=0)[..., None]
    before_im = jnp.concatenate([init[1][None], carried[3][:-1]], axis=0)[..., None]
    places = (jnp.arange(span, dtype=jnp.float32) + 1.0)[None, None, :]
    scaled = steps[:, :, None] * places
    magnitude = jnp.exp(a_re[None, :, None] * scaled)
    angle = a_im[None, :, None] * scaled
    lift_re = magnitude * jnp.cos(angle)
    lift_im = magnitude * jnp.sin(angle)
    state_re = inner_re + lift_re * before_re - lift_im * before_im
    state_im = inner_im + lift_re * before_im + lift_im * before_re
    highest = lax.Precision.HIGHEST
    response = jnp.einsum("cp,kps->ksc", out_map[0], state_re, precision=highest) - jnp.einsum(
        "cp,kps->ksc", out_map[1], state_im, precision=highest
    )
    response = response.reshape(length, series.shape[1]) + skip_row * series.astype(jnp.float32)
    return jax.nn.gelu(response).astype(jnp.bfloat16)


def mapper(left, piece):
    return jnp.dot(left, piece, preferred_element_type=jnp.float32)


def per_device(
    signal,
    pace,
    log_step,
    a_real,
    a_imag,
    in_map,
    out_map,
    skip,
    init_state,
    w_glu,
    b_glu,
    g_mix,
    w_out,
):
    local_seqs = signal.shape[0]
    tokens = signal.shape[1]
    width = signal.shape[2]
    groups = a_real.shape[0]
    channels = width // (groups * lax.axis_size(SP))
    grouped = lax.all_to_all(signal, SP, split_axis=2, concat_axis=1, tiled=True)
    length = grouped.shape[1]
    skips = skip.reshape(groups, channels)

    def per_sequence(inputs):
        sample, pace_row, init_row = inputs
        series = sample.reshape(length, groups, channels)
        outputs = jax.vmap(mix_group, in_axes=(1, None, 0, 0, 0, 0, 0, 0, 1), out_axes=1)(
            series, pace_row, log_step, a_real, a_imag, in_map, out_map, skips, init_row
        )
        return outputs.reshape(length, groups * channels)

    local_act = lax.map(per_sequence, (grouped, pace, init_state))
    activated = stepwise_exchange(local_act, SP, (0, 1), 1, 2)
    rows = activated.reshape(local_seqs * tokens, width)
    glu_full, out_full = in_one_piece((w_glu, w_out), SP, 0, 1)
    gate_pre = mapper(rows, gathered_copies(glu_full, "dp", 1)) + b_glu
    gated = rows.astype(jnp.float32) * jax.nn.sigmoid(gate_pre)
    scale = lax.rsqrt(jnp.mean(gated * gated, axis=-1, keepdims=True) + 1e-06)
    mixed = (gated * scale * g_mix).astype(jnp.bfloat16)
    output = mapper(mixed, lax.all_gather(out_full, "dp", axis=1, tiled=True)).astype(jnp.bfloat16)
    return output.reshape(local_seqs, tokens, output.shape[1])


def solution(mesh):
    split = Mesh(mesh.devices.reshape(16, 4, mesh.shape["dp"]), ("sp_0", "sp_1", "dp"))
    placed = (
        P("dp", SP, None),
        P("dp", None),
        P(SP),
        P(SP, None),
        P(SP, None),
        P(SP, None, None, None),
        P(SP, None, None, None),
        P(SP),
        P("dp", None, SP, None),
        P(SP, "dp"),
        P(),
        P(),
        P(SP, "dp"),
    )
    return jax.shard_map(
        per_device, mesh=split, in_specs=placed, out_specs=P("dp", SP, None), check_vma=False
    )
```

profile of v0, /device:TPU:1, one launch (start us, length us, event | category | flops | bytes accessed | tf_op | source)
XLA Modules:
  0.0 285.2 jit_solution(7003737996966265889)
XLA Ops:
  6.5 1.4 pad_maximum_fusion
  7.9 0.0 all-gather.3.cloned.1.call-update
  7.9 1.3 copy.37
  9.2 0.5 broadcast.2621
  9.8 2.2 reduce.14
  11.9 0.8 reshape.3159
  12.7 19.4 %all-to-all-start = ((bf16[64,2,1024]{2,1,0:T(2,128)(2,1)}), bf16[64,2,1024]{2,1,0:T(2,128)(2,1)S(1)}, u32[]{:S(2)}, u32[]{:S(2)}) async-start(bf16[64,2,1024]{2,1,0:T(2,128)(2,1)} %reshape.3159), calls=%async_computation | async-start | bytes 524288 | tf_op jit(solution)/shard_map/all_to_all | solution.py:143
  32.1 0.0 all-gather.5.cloned.1.call-start
  32.9 0.2 multiply_subtract_fusion.6
  33.2 113.9 %all-gather.3.cloned.1.call-done = bf16[1024,640]{1,0:T(8,128)(2,1)} async-done(((bf16[16,640]{1,0:T(8,128)(2,1)}), bf16[1024,640]{1,0:T(8,128)(2,1)}) %all-gather.3.cloned.1.call-update) | async-done | bytes 1310736 | tf_op jit(solution)/shard_map/all_gather | solution.py:37
  147.0 2.3 split.9
  149.3 0.0 all-gather.5.cloned.1.call-update
  149.5 0.1 broadcast_multiply_fusion
  149.6 0.2 multiply_subtract_fusion.13
  149.8 0.2 multiply_subtract_fusion.19
  150.1 0.1 subtract_convert_fusion
  150.2 0.2 reshape.3160
  150.5 1.4 convolution_bitcast_fusion
  151.9 0.6 fusion.66
  152.5 2.5 fusion.4
  155.1 2.5 multiply_subtract_fusion.5
  157.6 2.5 multiply_subtract_fusion.4
  160.1 2.5 multiply_subtract_fusion.3
  162.7 2.5 multiply_subtract_fusion.2
  165.2 2.5 multiply_subtract_fusion.1
  167.7 2.5 multiply_subtract_fusion
  170.3 0.2 slice_reduce_fusion.2
  170.4 0.2 slice_reduce_fusion.3
  170.6 1.0 copy-done
  171.6 1.2 slice_reduce_fusion
  172.8 0.2 scatter-add.9
  173.1 0.0 copy-start.8
  173.1 1.2 slice_reduce_fusion.1
  176.0 11.0 %fusion.5 = f32[64,128,16]{1,2,0:T(8,128)S(1)} fusion(f32[1,64,64,128]{3,2,1,0:T(8,128)} %copy-done, f32[64,64]{1,0:T(8,128)S(1)} %maximum_bitcast_fusion.1, f32[64,64]{1,0:T(8,128)S(1)} %maximum_bitcast_fusion, f32[64]{0:T(128)S(1)} %bitcast.139, f32[64,128]{1,0:T(8,128)S(1)} %broadcast_multiply_fusion, f32[64]{0:T(128)S(1)} %bitcast.144, ...), kind=kOutput, calls=%fused_computation.13 | convolution fusion | flops 104857600 | bytes 2728960 | tf_op jit(solution)/shard_map/while/body/eval_jaxpr/vmap(cp,kps->ksc)/dot_general | solution.py:112
  187.0 9.3 %fusion.21 = f32[64,128,16]{1,2,0:T(8,128)S(1)} fusion(f32[64,128,16]{1,2,0:T(8,128)S(1)} %fusion.5, f32[1,64,64,128]{3,2,1,0:T(8,128)S(1)} %get-tuple-element.74, f32[64,64]{1,0:T(8,128)S(1)} %maximum_bitcast_fusion.1, f32[64,64]{1,0:T(8,128)S(1)} %maximum_bitcast_fusion, f32[64]{0:T(128)S(1)} %bitcast.140, f32[64,128]{1,0:T(8,128)S(1)} %broadcast_multiply_fusion, ...), kind=kOutput, calls=%fused_computation.38 | convolution fusion | flops 104988672 | bytes 3253248 | tf_op jit(solution)/shard_map/while/body/eval_jaxpr/vmap(cp,kps->ksc)/dot_general | solution.py:112
  196.3 0.3 fusion.46
  196.6 19.1 %all_to_all.30 = bf16[16,4,1,128,16]{3,4,1,2,0:T(8,128)(2,1)S(1)} all-to-all(bf16[16,4,1,128,16]{3,4,1,2,0:T(8,128)(2,1)S(1)} %fusion.46), channel_id=1, replica_groups=mesh['sp_0'=16,'sp_1'=4,'dp'=8] {'sp_0'}, dimensions={0} | all-to-all | bytes 524288 | tf_op jit(solution)/shard_map/all_to_all | solution.py:25
  215.7 0.7 copy.40
  216.4 3.7 %all-to-all-start.2 = ((bf16[16,4,1,128,16]{3,4,0,2,1:T(8,128)(2,1)}), bf16[16,4,1,128,16]{3,4,0,2,1:T(8,128)(2,1)S(1)}, u32[]{:S(2)}, u32[]{:S(2)}) async-start(bf16[16,4,1,128,16]{3,4,0,2,1:T(8,128)(2,1)} %copy.40), calls=%async_computation.2 | async-start | bytes 524288 | tf_op jit(solution)/shard_map/all_to_all | solution.py:25
  220.1 0.1 copy.43
  220.3 5.7 %all-to-all-done.2 = bf16[16,4,1,128,16]{3,4,0,2,1:T(8,128)(2,1)S(1)} async-done(((bf16[16,4,1,128,16]{3,4,0,2,1:T(8,128)(2,1)}), bf16[16,4,1,128,16]{3,4,0,2,1:T(8,128)(2,1)S(1)}, u32[]{:S(2)}, u32[]{:S(2)}) %all-to-all-start.2) | async-done | bytes 262176 | tf_op jit(solution)/shard_map/all_to_all | solution.py:25
  225.9 1.6 broadcast_in_dim.18
  227.6 17.9 %all-to-all-start.3 = ((bf16[8,1024,128]{1,2,0:T(8,128)(2,1)}), bf16[8,1024,128]{1,2,0:T(8,128)(2,1)S(1)}, u32[]{:S(2)}, u32[]{:S(2)}) async-start(bf16[8,1024,128]{1,2,0:T(8,128)(2,1)} %broadcast_in_dim.18), calls=%async_computation.3 | async-start | bytes 4194304 | tf_op jit(solution)/shard_map/all_to_all | solution.py:43
  245.5 0.1 copy.42
  245.7 26.0 %all-to-all-done.3 = bf16[8,1024,128]{1,2,0:T(8,128)(2,1)S(1)} async-done(((bf16[8,1024,128]{1,2,0:T(8,128)(2,1)}), bf16[8,1024,128]{1,2,0:T(8,128)(2,1)S(1)}, u32[]{:S(2)}, u32[]{:S(2)}) %all-to-all-start.3) | async-done | bytes 2097184 | tf_op jit(solution)/shard_map/all_to_all | solution.py:43
  271.7 1.0 multiply_reduce_fusion
  272.7 0.0 all-gather.5.cloned.1.call-done
  272.7 5.7 %fusion = bf16[1,128,4096]{2,1,0:T(8,128)(2,1)} fusion(bf16[1024,4096]{1,0:T(8,128)(2,1)} %all-gather.5.cloned.1.call-done, f32[128,1024]{1,0:T(8,128)S(1)} %get-tuple-element.165, f32[1024]{0:T(1024)S(1)} %copy-done.1, f32[128]{0:T(128)S(1)} %add_rsqrt_fusion), kind=kOutput, calls=%fused_computation.1 | convolution fusion | flops 1074659328 | bytes 9966080 | tf_op jit(solution)/shard_map/dot_general | solution.py:120
  (148 shorter events, 1.6 us)
Async XLA Ops:
  6.5 26.3 %copy-start.7 = (f32[1,64]{1,0:T(1,128)S(1)}, f32[1,64]{1,0:T(1,128)}, u32[]{:S(2)}) copy-start(f32[1,64]{1,0:T(1,128)} %param.18) | copy-start | bytes 772
  6.5 26.3 %copy-start.4 = (f32[1,64]{1,0:T(1,128)S(1)}, f32[1,64]{1,0:T(1,128)}, u32[]{:S(2)}) copy-start(f32[1,64]{1,0:T(1,128)} %param.20) | copy-start | bytes 772
  6.5 26.4 %copy-start.3 = (f32[1,64]{1,0:T(1,128)S(1)}, f32[1,64]{1,0:T(1,128)}, u32[]{:S(2)}) copy-start(f32[1,64]{1,0:T(1,128)} %param.21) | copy-start | bytes 772
  6.5 140.5 %all-gather.3.cloned.1.call-start = ((), (), s32[]{:S(2)}) async-start(), calls=%async_computation.4 | async-start | bytes 1331200 | tf_op jit(solution)/shard_map/all_gather | solution.py:37
  11.9 137.4 %copy-start.5 = (f32[1,2,1,64]{3,2,1,0:T(1,128)S(1)}, f32[1,2,1,64]{3,2,1,0:T(1,128)}, u32[]{:S(2)}) copy-start(f32[1,2,1,64]{3,2,1,0:T(1,128)} %param.25) | copy-start | bytes 1540
  12.7 136.7 %copy-start.2 = (f32[1,2,64,16]{2,3,1,0:T(8,128)S(1)}, f32[1,2,64,16]{2,3,1,0:T(8,128)}, u32[]{:S(2)}) copy-start(f32[1,2,64,16]{2,3,1,0:T(8,128)} %param.22) | copy-start | bytes 24580
  12.7 137.5 %all-to-all-start = ((bf16[64,2,1024]{2,1,0:T(2,128)(2,1)}), bf16[64,2,1024]{2,1,0:T(2,128)(2,1)S(1)}, u32[]{:S(2)}, u32[]{:S(2)}) async-start(bf16[64,2,1024]{2,1,0:T(2,128)(2,1)} %reshape.3159), calls=%async_computation | async-start | bytes 524288 | tf_op jit(solution)/shard_map/all_to_all | solution.py:143
  32.1 240.6 %all-gather.5.cloned.1.call-start = ((), (), s32[]{:S(2)}) async-start(), calls=%async_computation.5 | async-start | bytes 9437184 | tf_op jit(solution)/shard_map/all_gather | solution.py:163
  170.3 1.4 copy-start
  173.1 2.9 %copy-start.8 = (f32[1,2,16,64]{3,2,1,0:T(8,128)S(1)}, f32[1,2,16,64]{3,2,1,0:T(8,128)}, u32[]{:S(2)}) copy-start(f32[1,2,16,64]{3,2,1,0:T(8,128)} %param.23) | copy-start | bytes 24580
  187.0 9.3 %copy-start.6 = (f32[16]{0:T(128)S(1)}, f32[16]{0:T(128)}, u32[]{:S(2)}) copy-start(f32[16]{0:T(128)} %param.24) | copy-start | bytes 196
  196.3 23.8 %slice-start = ((bf16[1024,640]{1,0:T(8,128)(2,1)}), bf16[1024,128]{1,0:T(8,128)(2,1)S(1)}, s32[]{:S(2)}) async-start(bf16[1024,640]{1,0:T(8,128)(2,1)} %all-gather.3.cloned.1.call-done), calls=%async_computation.6 | async-start | bytes 524288 | tf_op jit(solution)/shard_map/split | solution.py:38
  216.4 9.5 %all-to-all-start.2 = ((bf16[16,4,1,128,16]{3,4,0,2,1:T(8,128)(2,1)}), bf16[16,4,1,128,16]{3,4,0,2,1:T(8,128)(2,1)S(1)}, u32[]{:S(2)}, u32[]{:S(2)}) async-start(bf16[16,4,1,128,16]{3,4,0,2,1:T(8,128)(2,1)} %copy.40), calls=%async_computation.2 | async-start | bytes 524288 | tf_op jit(solution)/shard_map/all_to_all | solution.py:25
  227.6 44.1 %copy-start.9 = (f32[1024]{0:T(1024)S(1)}, f32[1024]{0:T(1024)}, u32[]{:S(2)}) copy-start(f32[1024]{0:T(1024)} %param.27) | copy-start | bytes 12292
  227.6 44.1 %all-to-all-start.3 = ((bf16[8,1024,128]{1,2,0:T(8,128)(2,1)}), bf16[8,1024,128]{1,2,0:T(8,128)(2,1)S(1)}, u32[]{:S(2)}, u32[]{:S(2)}) async-start(bf16[8,1024,128]{1,2,0:T(8,128)(2,1)} %broadcast_in_dim.18), calls=%async_computation.3 | async-start | bytes 4194304 | tf_op jit(solution)/shard_map/all_to_all | solution.py:43
  271.7 1.0 copy-start.1
Sparse Core Ops, SparseCore 0:
  10.3 136.6 all-gather.2
  149.4 63.6 all-gather.4
where the time goes:
time: 286 us; the launch traced here: 285 us
  waiting for transfers between devices  146 us (51%)
  starting transfers between devices  41 us (14%)
  matrix products  28.3 us (10%)
  other arithmetic  22.8 us (8%)
  blocking collectives  19.1 us (7%)
  between operations  14.8 us (5%)
  local copies, waits for them, and re-layouts  13.5 us (5%)
    all_gather x1, waiting for transfers between devices, in_one_piece(): whole = lax.all_gather(both, axis, axis=dim, tiled=True)  114 us
    all_to_all x1, waiting for transfers between devices, from_everyone(): return lax.all_to_all(copies, axis, split_axis=0, concat_axis=0, tiled=True)  26 us
    all_to_all x1, starting transfers between devices, per_device(): lax.all_to_all(signal, SP, split_axis=2, concat_axis=1, tiled=True)  19.4 us
    all_to_all x1, blocking collectives, moved_by_axis(): lax.all_to_all(pieces, axes[k], split_axis=k, concat_axis=k, tiled=True)  19.1 us
    all_to_all x1, starting transfers between devices, from_everyone(): return lax.all_to_all(copies, axis, split_axis=0, concat_axis=0, tiled=True)  17.9 us
    sub x7, other arithmetic, mix_group(): inner_re + power_re * moved_re - power_im * moved_im  17.7 us
    dot_general x1, matrix products, mix_group(): jnp.einsum('cp,kps->ksc', out_map[1], state_im, precision=highest)  11 us
    dot_general x1, matrix products, mix_group(): jnp.einsum('cp,kps->ksc', out_map[0], state_re, precision=highest)  9.28 us
  transfers between devices with their start and end apart: 5, of which 3 were waited for; matrix products, arithmetic and copies ran while one was open for 20% of the time, Pallas kernels for 0%

commit v1 on v0

v1 whole, which is shorter than its diff:
```python
import jax
import jax.numpy as jnp
from jax import lax
from jax.experimental import pallas as pl
from jax.experimental.pallas import tpu as pltpu
from jax.sharding import Mesh
from jax.sharding import PartitionSpec as P

NZ, NY, NX, NC = 16, 4, 4, 2
SPN = NZ * NY
SP = ("z", "y")
DP = ("x", "c")
HALF = NZ // 2
F32 = jnp.float32
BF16 = jnp.bfloat16
MESH = pl.DeviceIdType.MESH


def cmul(ar, ai, br, bi):
    return ar * br - ai * bi, ar * bi + ai * br


def body(
    sig, wg, wo, rhs_in, lhs_out, skip, step, are, aim, init, bglu, gmix,
    out,
    W, UT, U, Vr, Vi, ASend, ARecv, Br, Bi, mixed, gpre, obuf,
    loc, rps, rpr, rms, rmr, ays, ayr, axs, axr, ads, adr,
    bxs, bxr, bys, byr, bds, bdr, us, ur, vs, vr, osem,
):
    z = lax.axis_index("z")
    y = lax.axis_index("y")
    x = lax.axis_index("x")
    c = lax.axis_index("c")
    me = z * NY + y
    zp, zm = lax.rem(z + 1, NZ), lax.rem(z + NZ - 1, NZ)
    yp, ym, y2 = lax.rem(y + 1, NY), lax.rem(y + NY - 1, NY), lax.rem(y + 2, NY)
    xp, xm, x2 = lax.rem(x + 1, NX), lax.rem(x + NX - 1, NX), lax.rem(x + 2, NX)
    other = 1 - c

    def dev(zz=None, yy=None, xx=None, cc=None):
        return (
            z if zz is None else zz,
            y if yy is None else yy,
            x if xx is None else xx,
            c if cc is None else cc,
        )

    def rcopy(ref, ss, rs, to):
        return pltpu.make_async_remote_copy(
            src_ref=ref, dst_ref=ref, send_sem=ss, recv_sem=rs, device_id=to, device_id_type=MESH
        )

    barrier = pltpu.get_barrier_semaphore()

    def greet(d, carry):
        peer = lax.rem(me + d, SPN)
        pl.semaphore_signal(
            barrier, inc=1, device_id=dev(peer // NY, lax.rem(peer, NY)), device_id_type=MESH
        )
        return carry

    lax.fori_loop(1, SPN, greet, 0)
    for to in (dev(xx=xp), dev(xx=xm), dev(cc=other)):
        pl.semaphore_signal(barrier, inc=1, device_id=to, device_id_type=MESH)

    own = W.at[c, x, z, y]
    load_o = pltpu.make_async_copy(wo, own.at[:, pl.ds(0, 512)], loc.at[0])
    load_g = pltpu.make_async_copy(wg, own.at[:, pl.ds(512, 128)], loc.at[1])
    load_o.start()
    load_g.start()
    for b in range(8):
        piece = sig[0, :, b * 128 : (b + 1) * 128]
        UT[b * 8 : (b + 1) * 8] = piece.T.reshape(8, 16, 128)
    U[me] = UT[me]
    load_o.wait()
    load_g.wait()
    pl.semaphore_wait(barrier, SPN - 1 + 3)

    sent = []

    def push(copy):
        copy.start()
        sent.append(copy)

    def arrive(ref, rs):
        rcopy(ref, rs, rs, dev(cc=other)).wait_recv()

    def ring(t):
        za, zb = lax.rem(z + NZ - t, NZ), lax.rem(z + t, NZ)
        if 0 < t < HALF:
            arrive(W.at[c, x, za, y], rpr.at[t])
        if t < HALF - 1:
            push(rcopy(W.at[c, x, za, y], rps.at[t + 1], rpr.at[t + 1], dev(zz=zp)))
        if 0 < t <= HALF:
            arrive(W.at[c, x, zb, y], rmr.at[t])
        if t < HALF:
            push(rcopy(W.at[c, x, zb, y], rms.at[t + 1], rmr.at[t + 1], dev(zz=zm)))

    def around(i, view, plus, minus, at, ss, rs, stage):
        p_at, m_at, o_at = at
        if stage == 0:
            push(rcopy(view(None), ss.at[i, 0], rs.at[i, 0], plus))
            push(rcopy(view(None), ss.at[i, 1], rs.at[i, 1], minus))
        elif stage == 1:
            arrive(view(m_at), rs.at[i, 0])
            arrive(view(p_at), rs.at[i, 1])
            if i % 2 == 0:
                push(rcopy(view(m_at), ss.at[i, 2], rs.at[i, 2], plus))
            else:
                push(rcopy(view(p_at), ss.at[i, 2], rs.at[i, 2], minus))
        else:
            arrive(view(o_at), rs.at[i, 2])

    ysides = (dev(yy=yp), dev(yy=ym), (yp, ym, y2))
    xsides = (dev(xx=xp), dev(xx=xm), (xp, xm, x2))

    def chain_a(i, s):
        za = lax.rem(z + NZ - i, NZ)
        one = lambda at: W.at[c, x, za, y if at is None else at]
        row = lambda at: W.at[c, x if at is None else at, za]
        if s <= 1:
            around(i, one, *ysides, ays, ayr, s)
        elif s == 2:
            around(i, one, *ysides, ays, ayr, 2)
            around(i, row, *xsides, axs, axr, 0)
        elif s == 3:
            around(i, row, *xsides, axs, axr, 1)
        elif s == 4:
            around(i, row, *xsides, axs, axr, 2)
            push(rcopy(W.at[c, pl.ds(0, NX), za], ads.at[i], adr.at[i], dev(cc=other)))

    def chain_b(i, s):
        zb = lax.rem(z + 1 + i, NZ)
        one = lambda at: W.at[c, x if at is None else at, zb, y]
        col = lambda at: W.at[c, pl.ds(0, NX), zb, y if at is None else at]
        if s <= 1:
            around(i, one, *xsides, bxs, bxr, s)
        elif s == 2:
            around(i, one, *xsides, bxs, bxr, 2)
            around(i, col, *ysides, bys, byr, 0)
        elif s == 3:
            around(i, col, *ysides, bys, byr, 1)
        elif s == 4:
            around(i, col, *ysides, bys, byr, 2)
            push(rcopy(W.at[c, pl.ds(0, NX), zb], bds.at[i], bdr.at[i], dev(cc=other)))

    def advance(t):
        if t <= HALF:
            ring(t)
        for s in range(5):
            if 0 <= t - s < HALF:
                chain_a(t - s, s)
            if 0 <= t - 1 - s < HALF:
                chain_b(t - 1 - s, s)

    def to_peer(src, dst, ss, rs, peer):
        return pltpu.make_async_remote_copy(
            src_ref=src.at[peer],
            dst_ref=dst.at[me],
            send_sem=ss.at[peer],
            recv_sem=rs.at[me],
            device_id=dev(peer // NY, lax.rem(peer, NY)),
            device_id_type=MESH,
        )

    def from_peer(src, dst, ss, rs, peer):
        return pltpu.make_async_remote_copy(
            src_ref=src.at[peer],
            dst_ref=dst.at[peer],
            send_sem=ss.at[peer],
            recv_sem=rs.at[peer],
            device_id=dev(peer // NY, lax.rem(peer, NY)),
            device_id_type=MESH,
        )

    def every_peer(act):
        def one(d, carry):
            act(lax.rem(me + d, SPN))
            return carry

        lax.fori_loop(1, SPN, one, 0)

    advance(0)
    every_peer(lambda p: to_peer(UT, U, us, ur, p).start())
    for t in range(1, HALF + 1):
        advance(t)
    every_peer(lambda p: from_peer(UT, U, us, ur, p).wait_recv())

    st = step[...]
    decay = jnp.exp(are[...] * st)
    angle = aim[...] * st
    bar_r = decay * jnp.cos(angle)
    bar_i = decay * jnp.sin(angle)
    modulus = are[...] * are[...] + aim[...] * aim[...]
    co_r = ((bar_r - 1.0) * are[...] + bar_i * aim[...]) / modulus
    co_i = (bar_i * are[...] - (bar_r - 1.0) * aim[...]) / modulus

    def inject(a, carry):
        for j in range(8):
            r = a * 8 + j
            pair = jnp.concatenate([U[r], U[r + 32]], axis=0)
            v = lax.dot_general(
                pair, rhs_in[...], (((0,), (0,)), ((), ())), preferred_element_type=F32
            )
            Vr[a, :, j, :] = v[:, :128]
            Vi[a, :, j, :] = v[:, 128:]
        return carry

    lax.fori_loop(0, 4, inject, 0)

    def parts(m):
        return [m[a * 8 : (a + 1) * 8] for a in range(4)]

    bars = list(zip(parts(bar_r), parts(bar_i)))
    coefs = list(zip(parts(co_r), parts(co_i)))

    def first_pass(s8, carry):
        carry = list(carry)
        for q in range(8):
            s = s8 * 8 + q
            for a in range(4):
                zr, zi = cmul(*bars[a], *carry[a])
                carry[a] = (zr + Vr[a, s], zi + Vi[a, s])
        return tuple(carry)

    zero = jnp.zeros((8, 128), F32)
    ends = lax.fori_loop(0, 16, first_pass, ((zero, zero),) * 4)
    er = jnp.concatenate([e[0] for e in ends], axis=0)
    ei = jnp.concatenate([e[1] for e in ends], axis=0)
    er, ei = cmul(co_r, co_i, er, ei)
    pr, pi = bar_r, bar_i
    for _ in range(7):
        pr, pi = cmul(pr, pi, pr, pi)
    row = lax.broadcasted_iota(jnp.int32, (32, 128), 0)
    for d in (1, 2, 4, 8, 16):
        keep = row >= d
        qr, qi = pltpu.roll(pr, d, 0), pltpu.roll(pi, d, 0)
        fr, fi = pltpu.roll(er, d, 0), pltpu.roll(ei, d, 0)
        gr, gi = cmul(pr, pi, fr, fi)
        hr, hi = cmul(pr, pi, qr, qi)
        er, ei = jnp.where(keep, er + gr, er), jnp.where(keep, ei + gi, ei)
        pr, pi = jnp.where(keep, hr, pr), jnp.where(keep, hi, pi)
    ir = jnp.broadcast_to(init[0:1], (8, 128))
    ii = jnp.broadcast_to(init[1:2], (8, 128))
    lr, li = cmul(pr[31:32], pi[31:32], ir, ii)
    lr, li = pltpu.roll(lr + er[31:32], 64, 1), pltpu.roll(li + ei[31:32], 64, 1)
    low = lax.broadcasted_iota(jnp.int32, (8, 128), 1) < 64
    sr, si = jnp.where(low, ir, lr)[0:1], jnp.where(low, ii, li)[0:1]
    br, bi = cmul(pr, pi, sr, si)
    br, bi = pltpu.roll(br + er, 1, 0), pltpu.roll(bi + ei, 1, 0)
    first = row == 0
    Br[...] = jnp.where(first, sr, br)
    Bi[...] = jnp.where(first, si, bi)

    def second_pass(s8, carry):
        carry = list(carry)
        for q in range(8):
            s = s8 * 8 + q
            for a in range(4):
                vr_, vi_ = cmul(*coefs[a], Vr[a, s], Vi[a, s])
                zr, zi = cmul(*bars[a], *carry[a])
                zr, zi = zr + vr_, zi + vi_
                Vr[a, s] = zr
                Vi[a, s] = zi
                carry[a] = (zr, zi)
        return tuple(carry)

    start = tuple((Br[a * 8 : (a + 1) * 8], Bi[a * 8 : (a + 1) * 8]) for a in range(4))
    lax.fori_loop(0, 16, second_pass, start)

    def respond(a, carry):
        for j in range(8):
            r = a * 8 + j
            state = jnp.concatenate(
                [Vr[a, :, j, :].astype(BF16), Vi[a, :, j, :].astype(BF16)], axis=1
            )
            pair = jnp.concatenate([U[r], U[r + 32]], axis=0)
            v = lax.dot_general(
                lhs_out[...], state, (((1,), (1,)), ((), ())), preferred_element_type=F32
            )
            v = v + skip[...] * pair.astype(F32)
            v = jax.nn.gelu(v).astype(BF16)
            ASend[r] = v[:16]
            ASend[r + 32] = v[16:]
        return carry

    lax.fori_loop(0, 4, respond, 0)
    ARecv[me] = ASend[me]
    every_peer(lambda p: to_peer(ASend, ARecv, vs, vr, p).start())
    for t in range(HALF + 1, HALF + 6):
        advance(t)
    every_peer(lambda p: from_peer(ASend, ARecv, vs, vr, p).wait_recv())
    for i in range(HALF):
        za, zb = lax.rem(z + NZ - i, NZ), lax.rem(z + 1 + i, NZ)
        arrive(W.at[other, pl.ds(0, NX), za], adr.at[i])
        arrive(W.at[other, pl.ds(0, NX), zb], bdr.at[i])

    for b in range(8):
        piece = ARecv[b * 8 : (b + 1) * 8].reshape(128, 128)
        mixed[:, b * 128 : (b + 1) * 128] = piece.T
    for d in range(8):
        gpre[:, d * 128 : (d + 1) * 128] = jnp.dot(
            mixed[...],
            W[d % 2, d // 2, :, :, :, 512:640].reshape(1024, 128),
            preferred_element_type=F32,
        )
    gated = mixed[...].astype(F32) * jax.nn.sigmoid(gpre[...] + bglu[...])
    scale = lax.rsqrt(jnp.mean(gated * gated, axis=-1, keepdims=True) + 1e-06)
    mixed[...] = (gated * scale * gmix[...]).astype(BF16)
    stores = []
    for d in range(8):
        obuf[d] = jnp.dot(
            mixed[...],
            W[d % 2, d // 2, :, :, :, 0:512].reshape(1024, 512),
            preferred_element_type=F32,
        ).astype(BF16)
        copy = pltpu.make_async_copy(obuf.at[d], out.at[0, :, pl.ds(d * 512, 512)], osem.at[d])
        copy.start()
        stores.append(copy)
    every_peer(lambda p: to_peer(UT, U, us, ur, p).wait_send())
    every_peer(lambda p: to_peer(ASend, ARecv, vs, vr, p).wait_send())
    for copy in sent:
        copy.wait_send()
    for copy in stores:
        copy.wait()


def per_device(
    signal, pace, log_step, a_real, a_imag, in_map, out_map, skip, init_state, w_glu, b_glu, g_mix, w_out
):
    step = jnp.exp(log_step[0]) * pace[0]
    step = jnp.repeat(step.reshape(2, 32).T, 64, axis=1)
    are = jnp.tile(a_real, (1, 2))
    aim = jnp.tile(a_imag, (1, 2))
    eye = jnp.eye(2, dtype=F32)
    inside = in_map[0].astype(BF16).astype(F32)
    rhs_in = jnp.einsum("rpc,gh->gcrhp", inside, eye).reshape(32, 256).astype(BF16)
    signs = jnp.array([1.0, -1.0], F32)[:, None, None]
    lhs_out = jnp.einsum("rcp,gh->gcrhp", out_map[0] * signs, eye).reshape(32, 256).astype(BF16)
    skips = jnp.broadcast_to(jnp.tile(skip, 2)[:, None], (32, 128))
    init = jnp.pad(init_state[0, :, 0, :], ((0, 0), (0, 64)))
    dma = pltpu.SemaphoreType.DMA
    vmem = pl.BlockSpec(memory_space=pltpu.VMEM)
    anywhere = pl.BlockSpec(memory_space=pl.ANY)
    return pl.pallas_call(
        body,
        out_shape=jax.ShapeDtypeStruct((1, 128, 4096), BF16),
        in_specs=[vmem, anywhere, anywhere] + [vmem] * 9,
        out_specs=anywhere,
        scratch_shapes=[
            pltpu.VMEM((NC, NX, NZ, NY, 16, 640), BF16),
            pltpu.VMEM((SPN, 16, 128), BF16),
            pltpu.VMEM((SPN, 16, 128), BF16),
            pltpu.VMEM((4, 128, 8, 128), F32),
            pltpu.VMEM((4, 128, 8, 128), F32),
            pltpu.VMEM((SPN, 16, 128), BF16),
            pltpu.VMEM((SPN, 16, 128), BF16),
            pltpu.VMEM((32, 128), F32),
            pltpu.VMEM((32, 128), F32),
            pltpu.VMEM((128, 1024), BF16),
            pltpu.VMEM((128, 1024), F32),
            pltpu.VMEM((8, 128, 512), BF16),
            dma((2,)),
            dma((9,)), dma((9,)), dma((9,)), dma((9,)),
            dma((8, 3)), dma((8, 3)), dma((8, 3)), dma((8, 3)), dma((8,)), dma((8,)),
            dma((8, 3)), dma((8, 3)), dma((8, 3)), dma((8, 3)), dma((8,)), dma((8,)),
            dma((SPN,)), dma((SPN,)), dma((SPN,)), dma((SPN,)),
            dma((8,)),
        ],
        compiler_params=pltpu.CompilerParams(
            collective_id=0, has_side_effects=True, vmem_limit_bytes=48 * 1024 * 1024
        ),
    )(signal, w_glu, w_out, rhs_in, lhs_out, skips, step, are, aim, init, b_glu[None], g_mix[None])


def solution(mesh):
    split = Mesh(mesh.devices.reshape(NZ, NY, NX, NC), ("z", "y", "x", "c"))
    placed = (
        P(DP, SP, None),
        P(DP, None),
        P(SP),
        P(SP, None),
        P(SP, None),
        P(SP, None, None, None),
        P(SP, None, None, None),
        P(SP),
        P(DP, None, SP, None),
        P(SP, DP),
        P(),
        P(),
        P(SP, DP),
    )
    return jax.shard_map(
        per_device, mesh=split, in_specs=placed, out_specs=P(DP, SP, None), check_vma=False
    )
```

time: 286 us -> 99.3 us (0.35)
  waiting for transfers between devices: 146 us -> 0 us
  Pallas kernels: 0 us -> 90.6 us
  starting transfers between devices: 41 us -> 0 us
  matrix products: 28.3 us -> 0 us
  other arithmetic: 22.8 us -> 1.66 us
  blocking collectives: 19.1 us -> 0 us
  between operations: 14.8 us -> 0.81 us
  local copies, waits for them, and re-layouts: 13.5 us -> 5.73 us
    all_gather x2 -> x0, waiting for transfers between devices: 114 us -> none  [the longest x1 114 us: in_one_piece(): whole = lax.all_gather(both, axis, axis=dim, tiled=True)]
    pallas_call x0 -> x1, Pallas kernels: none -> 90.6 us  [per_device(): pl.pallas_call(body, out_shape=jax.ShapeDtypeStruct((1, 128, 4096), BF16)...]
    all_to_all x3 -> x0, starting transfers between devices: 41 us -> none  [the longest x1 19.4 us: per_device(): lax.all_to_all(signal, SP, split_axis=2, concat_axis=1, tiled=True)]
    all_to_all x3 -> x0, waiting for transfers between devices: 31.7 us -> none  [the longest x1 26 us: from_everyone(): return lax.all_to_all(copies, axis, split_axis=0, concat_axis=0, tiled=True)]
    dot_general x5 -> x0, matrix products: 28.3 us -> none  [the longest x1 11 us: mix_group(): jnp.einsum('cp,kps->ksc', out_map[1], state_im, precision=highest)]
    all_to_all x1 -> x0, blocking collectives: 19.1 us -> none  [moved_by_axis(): lax.all_to_all(pieces, axes[k], split_axis=k, concat_axis=k, tiled=True)]
    sub x12 -> x0, other arithmetic: 18.4 us -> none  [the longest x7 17.7 us: mix_group(): inner_re + power_re * moved_re - power_im * moved_im]
    slice x68 -> x0, local copies, waits for them, and re-layouts: 3.91 us -> none  [the longest x1 1.17 us: mix_group(): inner_re[:, :, -1].at[0]]
  transfers between devices with their start and end apart: 5 -> 0, of which waited for: 3 -> 0; matrix products, arithmetic and copies ran while one was open for 20% -> 0% of each run, Pallas kernels for 0% -> 0%
where the time goes in v1:
time: 99.3 us; the launch traced here: 98.8 us
  Pallas kernels  90.6 us (91%)
  local copies, waits for them, and re-layouts  5.73 us (6%)
  other arithmetic  1.66 us (2%)
    pallas_call x1, Pallas kernels, per_device(): pl.pallas_call(body, out_shape=jax.ShapeDtypeStruct((1, 128, 4096), BF16)...  90.6 us
    unnamed x13, local copies, waits for them, and re-layouts  2.19 us

profile of v1, /device:TPU:1, one launch (start us, length us, event | category | flops | bytes accessed | tf_op | source)
XLA Modules:
  0.0 98.8 jit_solution(8591317026667520913)
XLA Ops:
  0.0 0.0 copy-start
  0.7 0.7 multiply_reduce_fusion
  1.4 0.1 mul.22
  1.5 0.7 tile.30
  2.2 0.1 tile.31.are
  2.2 0.7 tile.33
  2.9 0.1 tile.34.aim
  3.0 0.7 tile.28
  3.6 0.1 broadcast_in_dim.17
  3.7 0.7 pad.4.init
  4.4 0.1 copy.17
  4.5 0.1 broadcast_in_dim.18.skip
  4.6 0.1 broadcast_in_dim.19
  4.7 0.1 reshape.33.step
  4.8 0.8 bitcast_multiply_fusion
  5.6 0.1 fusion.1
  5.7 0.0 copy-start.5
  5.7 0.1 convert_element_type.28.lhs_out
  5.8 0.6 copy-done.5
  6.4 0.1 fusion
  6.5 0.0 copy-start.1
  6.5 0.0 copy-start.2
  6.5 0.0 copy-start.3
  6.5 0.0 copy-start.4
  6.5 0.1 convert_element_type.25.rhs_in
  6.6 0.0 copy-done
  6.6 0.6 copy-done.1
  7.2 0.0 copy-done.2
  7.2 0.0 copy-done.3
  7.2 0.0 copy-done.4
  7.2 90.6 %shard_map.136 = bf16[1,128,4096]{2,1,0:T(8,128)(2,1)S(1)} custom-call(bf16[1,128,1024]{2,1,0:T(8,128)(2,1)S(1)} %copy-done, bf16[16,128]{1,0:T(8,128)(2,1)S(1)} %copy-done.2, bf16[16,512]{1,0:T(8,128)(2,1)S(1)} %copy-done.1, bf16[32,256]{1,0:T(8,128)(2,1)S(1)} %convert_element_type.25.rhs_in, bf16[32,256]{1,0:T(8,128)(2,1)S(1)} %convert_element_type.28.lhs_out, ...), custom_call_target="tpu_custom_call" | custom-call | tf_op jit(solution)/shard_map/pallas_call | solution.py:345
  97.9 1.0 copy.20
  (4 shorter events, 0.0 us)
Async XLA Ops:
  0.0 6.6 %copy-start = (bf16[1,128,1024]{2,1,0:T(8,128)(2,1)S(1)}, bf16[1,128,1024]{2,1,0:T(8,128)(2,1)}, u32[]{:S(2)}) copy-start(bf16[1,128,1024]{2,1,0:T(8,128)(2,1)} %sig.1) | copy-start | bytes 786436
  5.7 0.7 copy-start.5
  6.5 0.7 copy-start.1
  6.5 0.7 copy-start.2
  6.5 0.7 copy-start.3
  6.5 0.7 copy-start.4

commit v2 on v1

v2 whole, which is shorter than its diff:
```python
import jax
import jax.numpy as jnp
from jax import lax
from jax.experimental import pallas as pl
from jax.experimental.pallas import tpu as pltpu
from jax.sharding import Mesh
from jax.sharding import PartitionSpec as P

NZ, NY, NX, NC = 16, 4, 4, 2
SPN = NZ * NY
SP = ("z", "y")
DP = ("x", "c")
HALF = NZ // 2
F32 = jnp.float32
BF16 = jnp.bfloat16
MESH = pl.DeviceIdType.MESH


def cmul(ar, ai, br, bi):
    return ar * br - ai * bi, ar * bi + ai * br


def body(
    *args,
):
    inputs, out, copies, rest = args[:13], args[13], args[14:25], args[25:]
    body_of(*inputs[:3], *copies, inputs[3:], out, *rest)


def body_of(
    sig_hbm, wg, wo,
    sig, in_map, out_map, skip, pace, log_step, a_real, a_imag, init, bglu, gmix,
    small_hbm, out,
    W, UT, U, Vr, Vi, ASend, ARecv, Br, Bi, mixed, gpre, rows_in, rows_out, RJ, WJ, lanes,
    loc, sends, rpr, rmr, ayr, axr, bxr, byr, core, us, ur, vs, vr,
):
    z = lax.axis_index("z")
    y = lax.axis_index("y")
    x = lax.axis_index("x")
    c = lax.axis_index("c")
    me = z * NY + y
    zp, zm = lax.rem(z + 1, NZ), lax.rem(z + NZ - 1, NZ)
    yp, ym, y2 = lax.rem(y + 1, NY), lax.rem(y + NY - 1, NY), lax.rem(y + 2, NY)
    xp, xm, x2 = lax.rem(x + 1, NX), lax.rem(x + NX - 1, NX), lax.rem(x + 2, NX)
    other = 1 - c

    def dev(zz=None, yy=None, xx=None, cc=None):
        return (
            z if zz is None else zz,
            y if yy is None else yy,
            x if xx is None else xx,
            c if cc is None else cc,
        )

    def slot(zz, yy):
        return lax.rem(zz, HALF) * (2 * NY) + yy * 2 + zz // HALF

    def rcopy(ref, ss, rs, to):
        return pltpu.make_async_remote_copy(
            src_ref=ref, dst_ref=ref, send_sem=ss, recv_sem=rs, device_id=to, device_id_type=MESH
        )

    def every_peer(act):
        for dy in range(1, NY):
            act(z, lax.rem(y + dy, NY))

        def one(d, carry):
            zz = lax.rem(z + d, NZ)
            for dy in range(NY):
                act(zz, lax.rem(y + dy, NY))
            return carry

        lax.fori_loop(1, NZ, one, 0)

    load_sig = pltpu.make_async_copy(sig_hbm, sig, loc.at[2])
    load_sig.start()
    small = (in_map, out_map, skip, pace, log_step, a_real, a_imag, init, bglu, gmix)
    loads = []
    for n, (src, dst) in enumerate(zip(small_hbm, small, strict=True)):
        loads.append(pltpu.make_async_copy(src, dst, loc.at[3 + n]))
        loads[-1].start()
    barrier = pltpu.get_barrier_semaphore()

    def greet(to):
        pl.semaphore_signal(barrier, inc=1, device_id=to, device_id_type=MESH)

    with jax.named_scope("greet"):
        for to in (dev(xx=xp), dev(xx=xm), dev(cc=other)):
            greet(to)
        every_peer(lambda zz, yy: greet(dev(zz, yy)))

    with jax.named_scope("prepare"):
        own = W.at[c, x, z, y]
        load_o = pltpu.make_async_copy(wo, own.at[:, pl.ds(0, 512)], loc.at[0])
        load_g = pltpu.make_async_copy(wg, own.at[:, pl.ds(512, 128)], loc.at[1])
        load_o.start()
        load_g.start()
        load_sig.wait()
        for b in range(8):
            piece = sig[0, :, b * 128 : (b + 1) * 128]
            UT[b * 8 : (b + 1) * 8] = piece.T.reshape(8, 16, 128)
        U[slot(z, y)] = UT[me]
        for copy in loads:
            copy.wait()
        rows_in[...] = jnp.zeros((32, 256), F32)
        rows_out[...] = jnp.zeros((32, 256), F32)
        for g in range(2):
            for r in range(2):
                rs, cs = slice(g * 16, g * 16 + 16), slice(r * 128 + g * 64, r * 128 + g * 64 + 64)
                rows_in[rs, cs] = in_map[0, r]
                rows_out[rs, cs] = out_map[0, r] if r == 0 else -out_map[0, r]
            for n, ref in enumerate((a_real[0:1], a_imag[0:1], init[0, 0], init[0, 1])):
                lanes[n : n + 1, g * 64 : g * 64 + 64] = ref
        full_in = jnp.concatenate([rows_in[...]] * 8, axis=0)
        full_out = jnp.concatenate([rows_out[...]] * 8, axis=0).T
        row_of = lax.broadcasted_iota(jnp.int32, (256, 256), 0) // 32
        col_of = lax.broadcasted_iota(jnp.int32, (256, 256), 1) // 32
        for j in range(8):
            RJ[j] = jnp.where(row_of == j, full_in, 0.0).astype(BF16)
            WJ[j] = jnp.where(col_of == j, full_out, 0.0).astype(BF16)

        def column(line, count, offset):
            lane = lax.broadcasted_iota(jnp.int32, (count, line.shape[1]), 1)
            at = lax.broadcasted_iota(jnp.int32, (count, line.shape[1]), 0) + offset
            return jnp.sum(jnp.where(lane == at, line, 0.0), axis=1, keepdims=True)

        skips = jnp.broadcast_to(column(skip[...], 16, 0), (16, 128))[None]
        low32 = lax.broadcasted_iota(jnp.int32, (32, 128), 1) < 64
        line = pace[0:1]
        st = jnp.where(low32, column(line, 32, 0), column(line, 32, 32)) * jnp.exp(log_step[...])
        are, aim = lanes[0:1], lanes[1:2]
        decay = jnp.exp(are * st)
        angle = aim * st
        bar_r = decay * jnp.cos(angle)
        bar_i = decay * jnp.sin(angle)
        modulus = are * are + aim * aim
        co_r = ((bar_r - 1.0) * are + bar_i * aim) / modulus
        co_i = (bar_i * are - (bar_r - 1.0) * aim) / modulus
        pr, pi = bar_r, bar_i
        for _ in range(7):
            pr, pi = cmul(pr, pi, pr, pi)
    with jax.named_scope("barrier"):
        load_o.wait()
        load_g.wait()
        pl.semaphore_wait(barrier, SPN - 1 + 3)

    RING, NEAR, BULK, CORE = range(4)

    def push(ref, kind, rs, to):
        rcopy(ref, sends.at[kind], rs, to).start()

    def arrive(ref, rs):
        rcopy(ref, rs, rs, dev(cc=other)).wait_recv()

    def ring(t):
        za, zb = lax.rem(z + NZ - t, NZ), lax.rem(z + t, NZ)
        if 0 < t < HALF:
            arrive(W.at[c, x, za, y], rpr.at[t])
        if t < HALF - 1:
            push(W.at[c, x, za, y], RING, rpr.at[t + 1], dev(zz=zp))
        if 0 < t <= HALF:
            arrive(W.at[c, x, zb, y], rmr.at[t])
        if t < HALF:
            push(W.at[c, x, zb, y], RING, rmr.at[t + 1], dev(zz=zm))

    def around(i, view, pair, halves, kind, plus, minus, at, rs, stage):
        p_at, m_at, o_at = at
        if stage == 0:
            push(view(None), kind, rs.at[i, 0], plus)
            push(view(None), kind, rs.at[i, 0], minus)
        elif stage == 1:
            arrive(pair, rs.at[i, 0])
            push(halves[0](m_at), kind, rs.at[i, 1], plus)
            push(halves[1](p_at), kind, rs.at[i, 1], minus)
        else:
            arrive(view(o_at), rs.at[i, 1])

    ysides = (dev(yy=yp), dev(yy=ym), (yp, ym, y2))
    xsides = (dev(xx=xp), dev(xx=xm), (xp, xm, x2))

    def cut(view):
        return (
            lambda at: view(at).at[:, pl.ds(0, 384)],
            lambda at: view(at).at[:, pl.ds(384, 256)],
        )

    def chain_a(i, s):
        za = lax.rem(z + NZ - i, NZ)
        one = lambda at: W.at[c, x, za, y if at is None else at]
        row = lambda at: W.at[c, x if at is None else at, za]
        rows = (
            lambda at: W.at[c, at, za, pl.ds(0, 2)],
            lambda at: W.at[c, at, za, pl.ds(2, 2)],
        )
        if s <= 1:
            around(i, one, W.at[c, x, za, pl.ds(0, 2)], cut(one), NEAR, *ysides, ayr, s)
        elif s == 2:
            around(i, one, None, cut(one), NEAR, *ysides, ayr, 2)
            around(i, row, W.at[c, pl.ds(0, 2), za], rows, BULK, *xsides, axr, 0)
        elif s == 3:
            around(i, row, W.at[c, pl.ds(0, 2), za], rows, BULK, *xsides, axr, 1)
        elif s == 4:
            around(i, row, W.at[c, pl.ds(0, 2), za], rows, BULK, *xsides, axr, 2)
            push(W.at[c, pl.ds(0, NX), za], CORE, core.at[0], dev(cc=other))

    def chain_b(i, s):
        zb = lax.rem(z + 1 + i, NZ)
        one = lambda at: W.at[c, x if at is None else at, zb, y]
        col = lambda at: W.at[c, pl.ds(0, NX), zb, y if at is None else at]
        cols = (
            lambda at: W.at[c, pl.ds(0, 2), zb, at],
            lambda at: W.at[c, pl.ds(2, 2), zb, at],
        )
        if s <= 1:
            around(i, one, W.at[c, pl.ds(0, 2), zb, y], cut(one), NEAR, *xsides, bxr, s)
        elif s == 2:
            around(i, one, None, cut(one), NEAR, *xsides, bxr, 2)
            around(i, col, W.at[c, pl.ds(0, NX), zb, pl.ds(0, 2)], cols, BULK, *ysides, byr, 0)
        elif s == 3:
            around(i, col, W.at[c, pl.ds(0, NX), zb, pl.ds(0, 2)], cols, BULK, *ysides, byr, 1)
        elif s == 4:
            around(i, col, W.at[c, pl.ds(0, NX), zb, pl.ds(0, 2)], cols, BULK, *ysides, byr, 2)
            push(W.at[c, pl.ds(0, NX), zb], CORE, core.at[0], dev(cc=other))

    def advance(t):
        with jax.named_scope(f"t{t}"):
            if t <= HALF:
                ring(t)
            for s in range(5):
                if 0 <= t - s < HALF:
                    chain_a(t - s, s)
                if 0 <= t - 1 - s < HALF:
                    chain_b(t - 1 - s, s)

    def send_tile(src, dst, ss, rs, zz, yy):
        pltpu.make_async_remote_copy(
            src_ref=src,
            dst_ref=dst,
            send_sem=ss,
            recv_sem=rs,
            device_id=dev(zz, yy),
            device_id_type=MESH,
        ).start()

    def send_signal(dz):
        zz = lax.rem(z + dz + NZ, NZ)
        for dy in range(NY):
            if dz or dy:
                yy = lax.rem(y + dy, NY)
                send_tile(UT.at[zz * NY + yy], U.at[slot(z, y)], us.at[0], ur.at[0], zz, yy)

    def send_back(zz, yy):
        send_tile(ASend.at[slot(zz, yy)], ARecv.at[me], vs.at[0], vr.at[0], zz, yy)

    def all_tiles(ref, ss, rs):
        return rcopy(ref.at[pl.ds(0, SPN - 1)], ss, rs, dev(cc=other))

    for t, far in enumerate(((8,), (-7, 7), (-6, 6), (-5, 5), (-4, 4, -1, 1), (-3, 3, -2, 2, 0))):
        advance(t)
        with jax.named_scope("scatter"):
            for dz in far:
                send_signal(dz)
    advance(6)
    with jax.named_scope("await_signal"):
        all_tiles(U, us.at[0], ur.at[0]).wait_recv()

    with jax.named_scope("inject"):
        for a in range(4):
            for h in range(2):
                piece = U[a * 16 + h * 8 : a * 16 + h * 8 + 8].reshape(128, 128)
                mixed[:, a * 256 + h * 128 : a * 256 + h * 128 + 128] = piece.T

        def inject(a, carry):
            rows = mixed[:, pl.ds(pl.multiple_of(a * 256, 256), 256)]
            for j in range(8):
                v = jnp.dot(rows, RJ[j], preferred_element_type=F32)
                Vr[pl.ds(a * 1024 + j, 128, stride=8), :] = v[:, :128]
                Vi[pl.ds(a * 1024 + j, 128, stride=8), :] = v[:, 128:]
            return carry

        lax.fori_loop(0, 4, inject, 0)
    advance(7)

    def parts(m):
        return [m[a * 8 : (a + 1) * 8] for a in range(4)]

    bars = list(zip(parts(bar_r), parts(bar_i)))
    coefs = list(zip(parts(co_r), parts(co_i)))

    def first_pass(s8, carry):
        carry = list(carry)
        for q in range(8):
            s = s8 * 8 + q
            for a in range(4):
                at = pl.ds(pl.multiple_of(a * 1024 + s * 8, 8), 8)
                zr, zi = cmul(*bars[a], *carry[a])
                carry[a] = (zr + Vr[at], zi + Vi[at])
        return tuple(carry)

    zero = jnp.zeros((8, 128), F32)
    with jax.named_scope("first"):
        ends = lax.fori_loop(0, 16, first_pass, ((zero, zero),) * 4)
    er = jnp.concatenate([e[0] for e in ends], axis=0)
    ei = jnp.concatenate([e[1] for e in ends], axis=0)
    er, ei = cmul(co_r, co_i, er, ei)
    row = lax.broadcasted_iota(jnp.int32, (32, 128), 0)
    for d in (1, 2, 4, 8, 16):
        keep = row >= d
        qr, qi = pltpu.roll(pr, d, 0), pltpu.roll(pi, d, 0)
        fr, fi = pltpu.roll(er, d, 0), pltpu.roll(ei, d, 0)
        gr, gi = cmul(pr, pi, fr, fi)
        hr, hi = cmul(pr, pi, qr, qi)
        er, ei = jnp.where(keep, er + gr, er), jnp.where(keep, ei + gi, ei)
        pr, pi = jnp.where(keep, hr, pr), jnp.where(keep, hi, pi)
    ir = jnp.broadcast_to(lanes[2:3], (8, 128))
    ii = jnp.broadcast_to(lanes[3:4], (8, 128))
    lr, li = cmul(pr[31:32], pi[31:32], ir, ii)
    lr, li = pltpu.roll(lr + er[31:32], 64, 1), pltpu.roll(li + ei[31:32], 64, 1)
    low = lax.broadcasted_iota(jnp.int32, (8, 128), 1) < 64
    sr, si = jnp.where(low, ir, lr)[0:1], jnp.where(low, ii, li)[0:1]
    br, bi = cmul(pr, pi, sr, si)
    br, bi = pltpu.roll(br + er, 1, 0), pltpu.roll(bi + ei, 1, 0)
    Br[...] = jnp.where(row == 0, sr, br)
    Bi[...] = jnp.where(row == 0, si, bi)

    def second_pass(s8, carry):
        carry = list(carry)
        for q in range(8):
            s = s8 * 8 + q
            for a in range(4):
                at = pl.ds(pl.multiple_of(a * 1024 + s * 8, 8), 8)
                vr_, vi_ = cmul(*coefs[a], Vr[at], Vi[at])
                zr, zi = cmul(*bars[a], *carry[a])
                zr, zi = zr + vr_, zi + vi_
                Vr[at] = zr
                Vi[at] = zi
                carry[a] = (zr, zi)
        return tuple(carry)

    with jax.named_scope("second"):
        first = tuple((Br[a * 8 : (a + 1) * 8], Bi[a * 8 : (a + 1) * 8]) for a in range(4))
        lax.fori_loop(0, 16, second_pass, first)
    advance(8)

    with jax.named_scope("respond"):

        def respond(a, carry):
            total = jnp.zeros((128, 256), F32)
            for j in range(8):
                state = jnp.concatenate(
                    [ref[pl.ds(a * 1024 + j, 128, stride=8), :].astype(BF16) for ref in (Vr, Vi)], axis=1
                )
                total = total + jnp.dot(state, WJ[j], preferred_element_type=F32)
            for h in range(2):
                at = pl.ds(a * 16 + h * 8, 8)
                v = total[:, h * 128 : (h + 1) * 128].T.reshape(8, 16, 128)
                v = v + skips * U[at].astype(F32)
                ASend[at] = jax.nn.gelu(v).astype(BF16)
            return carry

        lax.fori_loop(0, 4, respond, 0)
    with jax.named_scope("scatter_back"):
        ARecv[me] = ASend[slot(z, y)]
        every_peer(send_back)
    for t in range(9, HALF + 6):
        advance(t)
    with jax.named_scope("await_activated"):
        all_tiles(ARecv, vs.at[0], vr.at[0]).wait_recv()
    with jax.named_scope("await_core"):
        arrive(W.at[other], core.at[0])

    with jax.named_scope("gate"):
        for b in range(8):
            piece = ARecv[b * 8 : (b + 1) * 8].reshape(128, 128)
            mixed[:, b * 128 : (b + 1) * 128] = piece.T
        for d in range(8):
            gpre[:, d * 128 : (d + 1) * 128] = jnp.dot(
                mixed[...],
                W[d % 2, d // 2, :, :, :, 512:640].reshape(1024, 128),
                preferred_element_type=F32,
            )
        gated = mixed[...].astype(F32) * jax.nn.sigmoid(gpre[...] + bglu[...])
        scale = lax.rsqrt(jnp.mean(gated * gated, axis=-1, keepdims=True) + 1e-06)
        mixed[...] = (gated * scale * gmix[...]).astype(BF16)
    with jax.named_scope("project"):
        for d in range(8):
            out[0, :, d * 512 : (d + 1) * 512] = jnp.dot(
                mixed[...],
                W[d % 2, d // 2, :, :, :, 0:512].reshape(1024, 512),
                preferred_element_type=F32,
            ).astype(BF16)
    with jax.named_scope("finish"):
        all_tiles(UT, us.at[0], ur.at[0]).wait_send()
        all_tiles(ASend, vs.at[0], vr.at[0]).wait_send()
        for ref, kind in (
            (W.at[0, pl.ds(0, 3), pl.ds(0, 5), 0], RING),
            (W.at[0, 0, pl.ds(0, 12)], NEAR),
            (W.at[0, pl.ds(0, 3)], BULK),
            (W.at[0], CORE),
        ):
            rcopy(ref, sends.at[kind], core.at[0], dev(cc=other)).wait_send()


def per_device(
    signal, pace, log_step, a_real, a_imag, in_map, out_map, skip, init_state, w_glu, b_glu, g_mix, w_out
):
    dma = pltpu.SemaphoreType.DMA
    anywhere = pl.BlockSpec(memory_space=pltpu.HBM)
    small = (
        jnp.swapaxes(in_map, 2, 3), out_map, skip[None], pace,
        log_step[None], a_real, a_imag, init_state, b_glu[None], g_mix[None],
    )
    return pl.pallas_call(
        body,
        out_shape=jax.ShapeDtypeStruct((1, 128, 4096), BF16),
        in_specs=[anywhere] * 13,
        out_specs=pl.BlockSpec(memory_space=pltpu.VMEM),
        scratch_shapes=[pltpu.VMEM(v.shape, v.dtype) for v in (signal, *small)]
        + [
            pltpu.VMEM((NC, NX, NZ, NY, 16, 640), BF16),
            pltpu.VMEM((SPN, 16, 128), BF16),
            pltpu.VMEM((SPN, 16, 128), BF16),
            pltpu.VMEM((4096, 128), F32),
            pltpu.VMEM((4096, 128), F32),
            pltpu.VMEM((SPN, 16, 128), BF16),
            pltpu.VMEM((SPN, 16, 128), BF16),
            pltpu.VMEM((32, 128), F32),
            pltpu.VMEM((32, 128), F32),
            pltpu.VMEM((128, 1024), BF16),
            pltpu.VMEM((128, 1024), F32),
            pltpu.VMEM((32, 256), F32),
            pltpu.VMEM((32, 256), F32),
            pltpu.VMEM((8, 256, 256), BF16),
            pltpu.VMEM((8, 256, 256), BF16),
            pltpu.VMEM((8, 128), F32),
            dma((13,)),
            dma((4,)),
            dma((9,)), dma((9,)),
            dma((8, 2)), dma((8, 2)), dma((8, 2)), dma((8, 2)),
            dma((1,)),
            dma((1,)), dma((1,)), dma((1,)), dma((1,)),
        ],
        compiler_params=pltpu.CompilerParams(
            collective_id=0, has_side_effects=True, vmem_limit_bytes=60 * 1024 * 1024
        ),
    )(signal, w_glu, w_out, *small)


def solution(mesh):
    split = Mesh(mesh.devices.reshape(NZ, NY, NX, NC), ("z", "y", "x", "c"))
    placed = (
        P(DP, SP, None),
        P(DP, None),
        P(SP),
        P(SP, None),
        P(SP, None),
        P(SP, None, None, None),
        P(SP, None, None, None),
        P(SP),
        P(DP, None, SP, None),
        P(SP, DP),
        P(),
        P(),
        P(SP, DP),
    )
    return jax.shard_map(
        per_device, mesh=split, in_specs=placed, out_specs=P(DP, SP, None), check_vma=False
    )
```

time: 99.3 us -> 76 us (0.77)
  Pallas kernels: 90.6 us -> 72.8 us
  local copies, waits for them, and re-layouts: 5.73 us -> 2.29 us
  other arithmetic: 1.66 us -> 0 us
    pallas_call x1, Pallas kernels: 90.6 us -> 72.8 us  [per_device(): pl.pallas_call(body, out_shape=jax.ShapeDtypeStruct((1, 128, 4096), BF16)...]
    another operation x6 -> x0, local copies, waits for them, and re-layouts: 2.15 us -> none  [the longest x2 0.74 us: per_device(): aim = jnp.tile(a_imag, (1, 2))]
    mul x2 -> x0, other arithmetic: 1.47 us -> none  [the longest x1 0.79 us: per_device(): out_map[0] * signs]
    unnamed x13 -> x1, local copies, waits for them, and re-layouts: 2.19 us -> 2.29 us
where the time goes in v2:
time: 76 us; the launch traced here: 75.8 us
  Pallas kernels  72.8 us (96%)
  local copies, waits for them, and re-layouts  2.29 us (3%)
    pallas_call x1, Pallas kernels, per_device(): pl.pallas_call(body, out_shape=jax.ShapeDtypeStruct((1, 128, 4096), BF16)...  72.8 us
    unnamed x1, local copies, waits for them, and re-layouts  2.29 us

profile of v2, /device:TPU:1, one launch (start us, length us, event | category | flops | bytes accessed | tf_op | source)
XLA Modules:
  0.0 75.8 jit_solution(5016155840025693524)
XLA Ops:
  0.7 72.8 %shard_map.127 = bf16[1,128,4096]{2,1,0:T(8,128)(2,1)} custom-call(bf16[1,128,1024]{2,1,0:T(8,128)(2,1)} %args_0_.4, bf16[16,128]{1,0:T(8,128)(2,1)} %args_1_.4, bf16[16,512]{1,0:T(8,128)(2,1)} %args_2_.4, f32[1,2,16,64]{3,2,1,0:T(8,128)} %bitcast.6, f32[1,2,16,64]{3,2,1,0:T(8,128)} %args_4_.4, f32[1,16]{1,0:T(1,128)} %bitcast.9, f32[1,64]{1,0:T(1,128)} %args_6_.4, ...), custom_call_target="tpu_custom_call" | custom-call | tf_op jit(solution)/shard_map/pallas_call | solution.py:413
  73.5 2.3 %copy.16 = bf16[1,128,4096]{2,1,0:T(8,128)(2,1)} copy(bf16[1,128,4096]{2,1,0:T(8,128)(2,1)} %shard_map.127) | data formatting | bytes 2097152
